TPU v7x, 32 devices: a whole 2x2x4 slice. The times are simulated.
32 devices in a mesh: sp: 8 (over z, x), tp: 4 (over y, core).
Axes of the slice: x: 2, y: 2, z: 4, core: 2. Of those that a mesh axis runs over, the one named last changes fastest.
Arguments:
- query_small: bfloat16 [6144, 1024], P('sp', 'tp'), may hold values from -6 to 6
- key_small: bfloat16 [6144, 1024], P('sp', 'tp'), may hold values from -6 to 6
- value_small: bfloat16 [6144, 1024], P('sp', 'tp'), may hold values from -6 to 6
- gates_small: float32 [6144, 16], P('sp', 'tp'), as said below
- query_large: bfloat16 [6144, 1024], P('sp', 'tp'), may hold values from -6 to 6
- key_large: bfloat16 [6144, 1024], P('sp', 'tp'), may hold values from -6 to 6
- value_large: bfloat16 [6144, 1024], P('sp', 'tp'), may hold values from -6 to 6
- gates_large: float32 [6144, 8], P('sp', 'tp'), as said below
- residual: bfloat16 [6144, 2048], P(('sp', 'tp')), may hold values from -6 to 6
- mixer_small: bfloat16 [1024, 2048], P('tp'), may hold values from -1 to 1
- mixer_large: bfloat16 [1024, 2048], P('tp'), may hold values from -1 to 1
- mix_gain: float32 [2048], replicated, may hold values from 0.1 to 1.9
- value_weight: bfloat16 [2048, 5632], P('sp', 'tp'), may hold values from -0.125 to 0.125
- gate_weight: bfloat16 [2048, 5632], P('sp', 'tp'), may hold values from -0.125 to 0.125
- value_taps: float32 [3, 5632], P(None, 'tp'), may hold values from -3 to 3
- gate_taps: float32 [3, 5632], P(None, 'tp'), may hold values from -3 to 3
- down_weight: bfloat16 [5632, 2048], P('tp', 'sp'), may hold values from -0.078125 to 0.078125
- final_gain: float32 [2048], replicated, may hold values from 0.1 to 1.9
Outputs:
- layer_out: bfloat16 [6144, 2048], P(('sp', 'tp'))
Inputs may be any that keep to these rules, and one draw needn't show every extreme that they name: `gates_small`: each column never rises from one position to the next, and its first entry is negative. `gates_large`: each column never rises from one position to the next, and its first entry is negative.
All inputs are finite; a program needn't handle non-finite values.
Results may differ from a plain program's by a relative error of at most 0.018.
Values may be sent and summed in bfloat16 or wider, within the bound.
A program may use at most 128 MiB of HBM per device.

v0:
```python
import math
import jax
import jax.numpy as jnp
from jax import lax
from jax.sharding import PartitionSpec as P

DS = 64
DL = 128
residual_scale = 2.0**0.5
epsilon = 1e-05


def passed_along(value, axis, steps):
    count = lax.axis_size(axis)
    first, last = (max(0, -steps), min(count, count - steps))
    return lax.ppermute(value, axis, [(source, source + steps) for source in range(first, last)])


def norm_rows(values, gain):
    center = jnp.mean(values, axis=-1, keepdims=True)
    spread = jnp.mean(jnp.square(values - center), axis=-1, keepdims=True)
    return (values - center) * lax.rsqrt(spread + epsilon) * gain


def attend_block(
    running,
    queries,
    query_gates,
    key_rows,
    value_rows,
    key_gates,
    token_positions,
    key_first,
    head_dim,
):
    running_peak, weight_sum, weighted = running
    heads_here = query_gates.shape[1]
    span_rows = key_rows.shape[0]
    query_heads = queries.reshape(queries.shape[0], heads_here, head_dim)
    key_heads = key_rows.reshape(span_rows, heads_here, head_dim)
    value_heads = value_rows.reshape(span_rows, heads_here, head_dim)
    scores = jnp.einsum(
        "qhd,khd->hqk", query_heads, key_heads, preferred_element_type=jnp.float32
    ) * head_dim ** (-0.5)
    scores = scores + query_gates.T[:, :, None] - key_gates.T[:, None, :]
    key_positions = key_first + jnp.arange(span_rows)
    allowed = token_positions[:, None] >= key_positions[None, :]
    scores = jnp.where(allowed[None], scores, -1e30)
    new_peak = jnp.maximum(running_peak, jnp.max(scores, axis=-1))
    factor = jnp.exp(running_peak - new_peak)
    weights = jnp.where(allowed[None], jnp.exp(scores - new_peak[:, :, None]), 0.0)
    weight_sum = weight_sum * factor + jnp.sum(weights, axis=-1)
    update = jnp.einsum(
        "hqk,khd->qhd",
        weights.astype(jnp.bfloat16),
        value_heads,
        preferred_element_type=jnp.float32,
    )
    weighted = weighted * factor.T[:, :, None] + update
    return (new_peak, weight_sum, weighted)


def per_device(
    query_small,
    key_small,
    value_small,
    gates_small,
    query_large,
    key_large,
    value_large,
    gates_large,
    residual,
    mixer_small,
    mixer_large,
    mix_gain,
    value_weight,
    gate_weight,
    value_taps,
    gate_taps,
    down_weight,
    final_gain,
):
    shard_rows = query_small.shape[0]
    first_row = lax.axis_index("sp") * shard_rows
    token_positions = first_row + jnp.arange(shard_rows)
    last_position = first_row + shard_rows - 1
    every_gate = (
        lax.all_gather(gates_small, "sp", axis=0, tiled=True),
        lax.all_gather(gates_large, "sp", axis=0, tiled=True),
    )
    heads_small = gates_small.shape[1]
    heads_large = gates_large.shape[1]

    def fresh(heads_here, head_dim):
        return (
            jnp.full((heads_here, shard_rows), -1e30, jnp.float32),
            jnp.zeros((heads_here, shard_rows), jnp.float32),
            jnp.zeros((shard_rows, heads_here, head_dim), jnp.float32),
        )

    pieces = (
        lax.all_gather(key_small, "sp", axis=0, tiled=True),
        lax.all_gather(value_small, "sp", axis=0, tiled=True),
        lax.all_gather(key_large, "sp", axis=0, tiled=True),
        lax.all_gather(value_large, "sp", axis=0, tiled=True),
    )
    span_total = pieces[0].shape[0]
    block_rows = shard_rows * math.gcd(span_total // shard_rows, max(1, 1024 // shard_rows))

    def one_block(block_index, current):
        offset = block_index * block_rows
        sliced = [lax.dynamic_slice_in_dim(member, offset, block_rows, 0) for member in pieces]
        gate_small = lax.dynamic_slice_in_dim(every_gate[0], offset, block_rows, 0)
        gate_large = lax.dynamic_slice_in_dim(every_gate[1], offset, block_rows, 0)

        def update(previous):
            return (
                attend_block(
                    previous[0],
                    query_small,
                    gates_small,
                    sliced[0],
                    sliced[1],
                    gate_small,
                    token_positions,
                    offset,
                    DS,
                ),
                attend_block(
                    previous[1],
                    query_large,
                    gates_large,
                    sliced[2],
                    sliced[3],
                    gate_large,
                    token_positions,
                    offset,
                    DL,
                ),
            )

        def unchanged(previous):
            return previous

        return lax.cond(offset <= last_position, update, unchanged, current)

    block_count = span_total // block_rows
    small_state, large_state = lax.fori_loop(
        0, block_count, one_block, (fresh(heads_small, DS), fresh(heads_large, DL))
    )
    small_out = (
        (small_state[2] / small_state[1].T[:, :, None])
        .reshape(shard_rows, heads_small * DS)
        .astype(jnp.bfloat16)
    )
    large_out = (
        (large_state[2] / large_state[1].T[:, :, None])
        .reshape(shard_rows, heads_large * DL)
        .astype(jnp.bfloat16)
    )
    tensor_parts = lax.axis_size("tp")
    own_rows = shard_rows // tensor_parts
    joined = jnp.concatenate([small_out, large_out], axis=1)
    arrived = lax.all_to_all(joined, "tp", split_axis=0, concat_axis=1, tiled=True)
    layout = arrived.reshape(own_rows, tensor_parts, joined.shape[1])
    small_width = small_out.shape[1]
    all_small = layout[:, :, :small_width].reshape(own_rows, tensor_parts * small_width)
    all_large = layout[:, :, small_width:].reshape(own_rows, tensor_parts * large_out.shape[1])
    mix = jnp.dot(
        all_small,
        lax.all_gather(mixer_small, "tp", axis=0, tiled=True),
        preferred_element_type=jnp.float32,
    ) + jnp.dot(
        all_large,
        lax.all_gather(mixer_large, "tp", axis=0, tiled=True),
        preferred_element_type=jnp.float32,
    )
    mixed = norm_rows(residual_scale * residual.astype(jnp.float32) + mix, mix_gain).astype(
        jnp.bfloat16
    )
    block_input = lax.all_gather(mixed, "tp", axis=0, tiled=True)

    def add_up(pieces):
        return (
            jnp.dot(block_input, pieces[0], preferred_element_type=jnp.float32),
            jnp.dot(block_input, pieces[1], preferred_element_type=jnp.float32),
        )

    up_value, up_gate = add_up(
        (
            lax.all_gather(value_weight, "sp", axis=0, tiled=True),
            lax.all_gather(gate_weight, "sp", axis=0, tiled=True),
        )
    )
    up_value = up_value.astype(jnp.bfloat16)
    up_gate = up_gate.astype(jnp.bfloat16)
    hidden_width = up_value.shape[1]
    trailing = jnp.concatenate([up_value[-2:], up_gate[-2:]], axis=1)
    earlier = passed_along(trailing, "sp", 1)
    padded_value = jnp.concatenate([earlier[:, :hidden_width], up_value], axis=0).astype(
        jnp.float32
    )
    padded_gate = jnp.concatenate([earlier[:, hidden_width:], up_gate], axis=0).astype(jnp.float32)
    filt_value = (
        value_taps[0] * padded_value[:-2]
        + value_taps[1] * padded_value[1:-1]
        + value_taps[2] * padded_value[2:]
    )
    filt_gate = (
        gate_taps[0] * padded_gate[:-2]
        + gate_taps[1] * padded_gate[1:-1]
        + gate_taps[2] * padded_gate[2:]
    )
    hidden = (jax.nn.silu(filt_gate) * filt_value).astype(jnp.bfloat16)
    ffn_terms = jnp.dot(
        hidden,
        lax.all_gather(down_weight, "sp", axis=1, tiled=True),
        preferred_element_type=jnp.float32,
    )
    ffn = lax.psum_scatter(
        ffn_terms.astype(jnp.bfloat16), "tp", scatter_dimension=0, tiled=True
    ).astype(jnp.float32)
    return norm_rows(residual_scale * mixed.astype(jnp.float32) + ffn, final_gain).astype(
        jnp.bfloat16
    )


def solution(mesh):
    in_specs = (
        P("sp", "tp"),
        P("sp", "tp"),
        P("sp", "tp"),
        P("sp", "tp"),
        P("sp", "tp"),
        P("sp", "tp"),
        P("sp", "tp"),
        P("sp", "tp"),
        P(("sp", "tp"), None),
        P("tp", None),
        P("tp", None),
        P(),
        P("sp", "tp"),
        P("sp", "tp"),
        P(None, "tp"),
        P(None, "tp"),
        P("tp", "sp"),
        P(),
    )
    out_specs = P(("sp", "tp"), None)
    return jax.shard_map(
        per_device, mesh=mesh, in_specs=in_specs, out_specs=out_specs, check_vma=False
    )
```

profile of v0, /device:TPU:0, one launch (start us, length us, event | category | flops | bytes accessed | tf_op | source)
XLA Modules:
  0.0 712.8 jit_solution(5404534390486293177)
XLA Ops:
  16.8 33.1 %all_gather.40 = f32[6144,2]{0,1:T(2,128)S(1)} all-gather(f32[768,2]{0,1:T(2,128)S(1)} %copy-done.5), channel_id=1, replica_groups=mesh['sp'=8,'tp'=4] {'sp'}, dimensions={0}, use_global_device_ids=true | all-gather | bytes 55296 | tf_op jit(solution)/shard_map/all_gather | solution.py:89
  49.9 31.3 %all_gather.37 = f32[6144,4]{0,1:T(4,128)S(1)} all-gather(f32[768,4]{0,1:T(4,128)S(1)} %copy-done.3), channel_id=1, replica_groups=mesh['sp'=8,'tp'=4] {'sp'}, dimensions={0}, use_global_device_ids=true | all-gather | bytes 110592 | tf_op jit(solution)/shard_map/all_gather | solution.py:88
  81.2 53.8 %all-gather.13.cloned.1.call-done = bf16[6144,256]{0,1:T(8,128)(2,1)} async-done(((bf16[768,256]{0,1:T(8,128)(2,1)}), bf16[6144,256]{0,1:T(8,128)(2,1)}) %all-gather.13.cloned.1.call-update) | async-done | bytes 3145744 | tf_op jit(solution)/shard_map/all_gather | solution.py:103
  135.0 61.0 %all-gather.15.cloned.1.call-done = bf16[6144,256]{0,1:T(8,128)(2,1)} async-done(((bf16[768,256]{0,1:T(8,128)(2,1)}), bf16[6144,256]{0,1:T(8,128)(2,1)}) %all-gather.15.cloned.1.call-update) | async-done | bytes 3145744 | tf_op jit(solution)/shard_map/all_gather | solution.py:104
  196.0 60.8 %all-gather.17.cloned.1.call-done = bf16[6144,256]{0,1:T(8,128)(2,1)} async-done(((bf16[768,256]{0,1:T(8,128)(2,1)}), bf16[6144,256]{0,1:T(8,128)(2,1)}) %all-gather.17.cloned.1.call-update) | async-done | bytes 3145744 | tf_op jit(solution)/shard_map/all_gather | solution.py:105
  257.0 19.2 %while.24 = (s32[]{:T(128)}, f32[4,768]{1,0:T(4,128)S(1)}, f32[4,768]{1,0:T(4,128)S(1)}, f32[768,4,64]{0,2,1:T(8,128)S(1)}, f32[2,768]{1,0:T(2,128)S(1)}, /*inde...) while((s32[]{:T(128)}, f32[4,768]{1,0:T(4,128)S(1)}, ...), condition=%wide.region_7.8_spmd.clone, body=%wide.region_0.7_spmd.clone.sunk | while | flops 1276591104 | bytes 55708176 | solution.py:148
  257.0 18.5 %conditional.3 = ((f32[4,768]{1,0:T(4,128)S(1)}, f32[4,768]{1,0:T(4,128)S(1)}, f32[768,4,64]{0,2,1:T(8,128)S(1)}, f32[2,768]{1,0:T(2,128)S(1)}, f32[2,768]{1,0:T(2,128)S(1)}, /*index=5*/f32[768,2,128]{2,0,1:T(8,128)S(1)})) conditional(s32[]{:T(128)} %convert_element_type.127, (f32[4,768]{1,0:T(4,128)S(1)}, f32[4,768]{1,0:T(4,128)S(1)}, ...), branch_computations={%region_1.0_spmd, %region_2.6_spmd} | conditional | flops 1276591104 | bytes 55704688 | solution.py:145
  260.2 2.5 fusion.20
  265.7 2.7 fusion.4
  268.5 3.6 fusion.23
  272.1 3.5 fusion.3
  279.1 19.0 %all_to_all.13 = bf16[4,192,512]{2,1,0:T(8,128)(2,1)S(1)} all-to-all(bf16[4,192,512]{2,1,0:T(8,128)(2,1)S(1)} %copy.51), channel_id=1, replica_groups=mesh['sp'=8,'tp'=4] {'tp'}, dimensions={0} | all-to-all | bytes 1572864 | tf_op jit(solution)/shard_map/all_to_all | solution.py:164
  298.3 3.5 fusion.49
  301.8 26.2 %all-gather.21.cloned.1.call-done = bf16[1024,2048]{1,0:T(8,128)(2,1)} async-done(((bf16[256,2048]{1,0:T(8,128)(2,1)}), bf16[1024,2048]{1,0:T(8,128)(2,1)}) %all-gather.21.cloned.1.call-update) | async-done | bytes 4194320 | tf_op jit(solution)/shard_map/all_gather | solution.py:175
  328.0 3.6 fusion.48
  334.5 92.2 %all-gather.25.cloned.1.call-done = bf16[2048,1408]{1,0:T(8,128)(2,1)} async-done(((bf16[256,1408]{1,0:T(8,128)(2,1)}), bf16[2048,1408]{1,0:T(8,128)(2,1)}) %all-gather.25.cloned.1.call-update) | async-done | bytes 5767184 | tf_op jit(solution)/shard_map/all_gather | solution.py:191
  426.7 30.9 %all-gather.23.cloned.1.call-done = bf16[768,2048]{1,0:T(8,128)(2,1)} async-done(((bf16[192,2048]{1,0:T(8,128)(2,1)}), bf16[768,2048]{1,0:T(8,128)(2,1)}) %all-gather.23.cloned.1.call-update) | async-done | bytes 3145744 | tf_op jit(solution)/shard_map/all_gather | solution.py:181
  457.6 8.3 %convolution_convert_fusion.2 = bf16[768,1408]{1,0:T(8,128)(2,1)S(1)} fusion(bf16[768,2048]{1,0:T(8,128)(2,1)} %all-gather.23.cloned.1.call-done, bf16[2048,1408]{1,0:T(8,128)(2,1)} %all-gather.25.cloned.1.call-done), kind=kOutput, calls=%fused_computation.57 | convolution fusion | flops 4430266368 | bytes 11075584 | tf_op jit(solution)/shard_map/dot_general | solution.py:185
  467.3 84.8 %all-gather.27.cloned.1.call-done = bf16[2048,1408]{1,0:T(8,128)(2,1)} async-done(((bf16[256,1408]{1,0:T(8,128)(2,1)}), bf16[2048,1408]{1,0:T(8,128)(2,1)}) %all-gather.27.cloned.1.call-update) | async-done | bytes 5767184 | tf_op jit(solution)/shard_map/all_gather | solution.py:192
  552.1 8.5 %convolution_convert_fusion.1 = bf16[768,1408]{1,0:T(8,128)(2,1)S(1)} fusion(bf16[768,2048]{1,0:T(8,128)(2,1)} %all-gather.23.cloned.1.call-done, bf16[2048,1408]{1,0:T(8,128)(2,1)} %all-gather.27.cloned.1.call-done), kind=kOutput, calls=%fused_computation.56 | convolution fusion | flops 4430266368 | bytes 11075584 | tf_op jit(solution)/shard_map/dot_general | solution.py:186
  564.6 4.2 maximum_convert_fusion
  568.9 76.7 %all-gather.29.cloned.1.call-done = bf16[1408,2048]{1,0:T(8,128)(2,1)} async-done(((bf16[1408,256]{1,0:T(8,128)(2,1)}), bf16[1408,2048]{1,0:T(8,128)(2,1)}) %all-gather.29.cloned.1.call-update) | async-done | bytes 5767184 | tf_op jit(solution)/shard_map/all_gather | solution.py:217
  645.6 19.1 %convolution_convert_fusion = bf16[768,2048]{1,0:T(8,128)(2,1)} fusion(bf16[1408,2048]{1,0:T(8,128)(2,1)} %all-gather.29.cloned.1.call-done, f32[770,1408]{1,0:T(8,128)} %get-tuple-element.726, f32[770,1408]{1,0:T(8,128)} %get-tuple-element.725, f32[1408]{0:T(1024)S(1)} %get-tuple-element.665, f32[1408]{0:T(1024)S(1)} %get-tuple-element.666, ...), kind=kOutput, calls=%fused_computation.55 | convolution fusion | flops 4448059392 | bytes 34898944 | tf_op jit(solution)/shard_map/dot_general | solution.py:215
  664.7 36.2 %reduce-scatter.2.cloned.1.call-done = bf16[192,2048]{1,0:T(8,128)(2,1)} async-done(((bf16[768,2048]{1,0:T(8,128)(2,1)}), bf16[192,2048]{1,0:T(8,128)(2,1)}) %reduce-scatter.2.cloned.1.call-update) | async-done | bytes 786448 | tf_op jit(solution)/shard_map/reduce_scatter | solution.py:220
  (112 shorter events, 33.0 us)
Async XLA Ops:
  6.5 10.1 %copy-start.4 = (bf16[768,256]{1,0:T(8,128)(2,1)S(1)}, bf16[768,256]{1,0:T(8,128)(2,1)}, u32[]{:S(2)}) copy-start(bf16[768,256]{1,0:T(8,128)(2,1)} %param.22) | copy-start | bytes 1179652
  6.5 10.2 %copy-start.5 = (f32[768,2]{0,1:T(2,128)S(1)}, f32[768,2]{0,1:T(2,128)}, u32[]{:S(2)}) copy-start(f32[768,2]{0,1:T(2,128)} %param.29) | copy-start | bytes 18436
  6.5 43.4 %copy-start.3 = (f32[768,4]{0,1:T(4,128)S(1)}, f32[768,4]{0,1:T(4,128)}, u32[]{:S(2)}) copy-start(f32[768,4]{0,1:T(4,128)} %param.25) | copy-start | bytes 36868
  6.5 74.7 %all-gather.11.cloned.1.call-start = ((), (), s32[]{:S(2)}) async-start(), calls=%async_computation.2 | async-start | bytes 3538944 | tf_op jit(solution)/shard_map/all_gather | solution.py:102
  8.5 248.5 %copy-start.10 = (bf16[768,256]{1,0:T(8,128)(2,1)S(1)}, bf16[768,256]{1,0:T(8,128)(2,1)}, u32[]{:S(2)}) copy-start(bf16[768,256]{1,0:T(8,128)(2,1)} %param.26) | copy-start | bytes 1179652
  8.5 126.5 %all-gather.13.cloned.1.call-start = ((), (), s32[]{:S(2)}) async-start(), calls=%async_computation.3 | async-start | bytes 3538944 | tf_op jit(solution)/shard_map/all_gather | solution.py:103
  10.6 185.4 %all-gather.15.cloned.1.call-start = ((), (), s32[]{:S(2)}) async-start(), calls=%async_computation.4 | async-start | bytes 3538944 | tf_op jit(solution)/shard_map/all_gather | solution.py:104
  12.6 244.2 %all-gather.17.cloned.1.call-start = ((), (), s32[]{:S(2)}) async-start(), calls=%async_computation.5 | async-start | bytes 3538944 | tf_op jit(solution)/shard_map/all_gather | solution.py:105
  14.6 283.6 %all-gather.19.cloned.1.call-start = ((), (), s32[]{:S(2)}) async-start(), calls=%async_computation.6 | async-start | bytes 5242880 | tf_op jit(solution)/shard_map/all_gather | solution.py:171
  15.2 312.8 %all-gather.21.cloned.1.call-start = ((), (), s32[]{:S(2)}) async-start(), calls=%async_computation.7 | async-start | bytes 5242880 | tf_op jit(solution)/shard_map/all_gather | solution.py:175
  15.8 410.9 %all-gather.25.cloned.1.call-start = ((), (), s32[]{:S(2)}) async-start(), calls=%async_computation.9 | async-start | bytes 6488064 | tf_op jit(solution)/shard_map/all_gather | solution.py:191
  16.5 441.0 %all-gather.23.cloned.1.call-start = ((), (), s32[]{:S(2)}) async-start(), calls=%async_computation.8 | async-start | bytes 3932160 | tf_op jit(solution)/shard_map/all_gather | solution.py:181
  328.0 3.9 copy-start.6
  333.1 218.9 %all-gather.27.cloned.1.call-start = ((), (), s32[]{:S(2)}) async-start(), calls=%async_computation.10 | async-start | bytes 6488064 | tf_op jit(solution)/shard_map/all_gather | solution.py:192
  333.9 311.7 %all-gather.29.cloned.1.call-start = ((), (), s32[]{:S(2)}) async-start(), calls=%async_computation.11 | async-start | bytes 6488064 | tf_op jit(solution)/shard_map/all_gather | solution.py:217
  334.5 366.5 %reduce-scatter.2.cloned.1.call-start = ((), (), s32[]{:S(2)}) async-start(), calls=%async_computation.12 | async-start | bytes 3932160 | tf_op jit(solution)/shard_map/reduce_scatter | solution.py:220
  465.9 1.4 copy-start.1
  467.3 95.8 %copy-start.7 = (f32[3,1408]{1,0:T(4,128)S(1)}, f32[3,1408]{1,0:T(4,128)}, u32[]{:S(2)}) copy-start(f32[3,1408]{1,0:T(4,128)} %param.36) | copy-start | bytes 50692
  467.3 95.8 %copy-start.8 = (f32[3,1408]{1,0:T(4,128)S(1)}, f32[3,1408]{1,0:T(4,128)}, u32[]{:S(2)}) copy-start(f32[3,1408]{1,0:T(4,128)} %param.37) | copy-start | bytes 50692
  552.1 12.6 %copy-start.2 = (bf16[768,1408]{1,0:T(8,128)(2,1)S(1)}, bf16[768,1408]{1,0:T(8,128)(2,1)}, u32[]{:S(2)}) copy-start(bf16[768,1408]{1,0:T(8,128)(2,1)} %copy-done.1) | copy-start | bytes 6488068
  560.6 4.0 collective-permute-start
  664.7 39.7 %copy-start.9 = (f32[2048]{0:T(1024)S(1)}, f32[2048]{0:T(1024)}, u32[]{:S(2)}) copy-start(f32[2048]{0:T(1024)} %param.39) | copy-start | bytes 24580
  700.9 3.5 copy-start
Sparse Core Ops, SparseCore 0:
  9.6 64.2 all-gather.10
  76.1 58.8 all-gather.12
  137.3 58.6 all-gather.14
  198.1 58.6 all-gather.16
  258.2 37.8 all-gather.18
  297.5 30.4 all-gather.20
  330.2 96.4 all-gather.24
  428.2 29.2 all-gather.22
  459.7 92.2 all-gather.26
  554.0 91.6 all-gather.28
  664.8 36.0 reduce-scatter.1
where the time goes:
time: 714 us; the launch traced here: 713 us
  waiting for transfers between devices  527 us (74%)
  blocking collectives  83.4 us (12%)
  matrix products  53.3 us (7%)
  other arithmetic  17.8 us (2%)
  local copies, waits for them, and re-layouts  14 us (2%)
  between operations  13.6 us (2%)
    all_gather x1, waiting for transfers between devices, per_device(): lax.all_gather(value_weight, 'sp', axis=0, tiled=True)  92.2 us
    all_gather x1, waiting for transfers between devices, per_device(): lax.all_gather(gate_weight, 'sp', axis=0, tiled=True)  84.8 us
    all_gather x1, waiting for transfers between devices, per_device(): lax.all_gather(down_weight, 'sp', axis=1, tiled=True)  76.7 us
    all_gather x1, waiting for transfers between devices, per_device(): lax.all_gather(key_large, 'sp', axis=0, tiled=True)  61 us
    all_gather x1, waiting for transfers between devices, per_device(): lax.all_gather(value_large, 'sp', axis=0, tiled=True)  60.8 us
    all_gather x1, waiting for transfers between devices, per_device(): lax.all_gather(value_small, 'sp', axis=0, tiled=True)  53.8 us
    reduce_scatter x1, waiting for transfers between devices, per_device(): lax.psum_scatter(ffn_terms.astype(jnp.bfloat16), 'tp', scatter_dimension=...  36.2 us
    all_gather x1, blocking collectives, per_device(): lax.all_gather(gates_large, 'sp', axis=0, tiled=True)  33.1 us
  transfers between devices with their start and end apart: 12, of which 10 were waited for; matrix products, arithmetic and copies ran while one was open for 8% of the time, Pallas kernels for 0%

commit v1 on v0

--- a/solution.py
+++ b/solution.py
@@ -8,6 +8,12 @@
 DL = 128
 residual_scale = 2.0**0.5
 epsilon = 1e-05
+
+
+def gathered_along(value, axis, d):
+    parts = lax.all_gather(value, axis, axis=0, tiled=False)
+    whole = jnp.concatenate(parts, axis=d)
+    return whole
 
 
 def passed_along(value, axis, steps):
@@ -213,9 +219,7 @@
     )
     hidden = (jax.nn.silu(filt_gate) * filt_value).astype(jnp.bfloat16)
     ffn_terms = jnp.dot(
-        hidden,
-        lax.all_gather(down_weight, "sp", axis=1, tiled=True),
-        preferred_element_type=jnp.float32,
+        hidden, gathered_along(down_weight, "sp", 1), preferred_element_type=jnp.float32
     )
     ffn = lax.psum_scatter(
         ffn_terms.astype(jnp.bfloat16), "tp", scatter_dimension=0, tiled=True

time: 714 us -> 726 us (1.017)
  local copies, waits for them, and re-layouts: 14 us -> 23.6 us
    reshape x0 -> x1, local copies, waits for them, and re-layouts: none -> 8.26 us  [gathered_along(): whole = jnp.concatenate(parts, axis=d)]
  transfers between devices with their start and end apart: 12 -> 12, of which waited for: 10 -> 9; matrix products, arithmetic and copies ran while one was open for 8% -> 8% of each run, Pallas kernels for 0% -> 0%
where the time goes in v1:
time: 726 us; the launch traced here: 725 us
  waiting for transfers between devices  529 us (73%)
  blocking collectives  83.4 us (11%)
  matrix products  51.9 us (7%)
  local copies, waits for them, and re-layouts  23.6 us (3%)
  other arithmetic  20.1 us (3%)
  between operations  13.6 us (2%)
    all_gather x1, waiting for transfers between devices, per_device(): lax.all_gather(value_weight, 'sp', axis=0, tiled=True)  92.1 us
    all_gather x1, waiting for transfers between devices, per_device(): lax.all_gather(gate_weight, 'sp', axis=0, tiled=True)  84.8 us
    all_gather x1, waiting for transfers between devices, gathered_along(): parts = lax.all_gather(value, axis, axis=0, tiled=False)  80.5 us
    all_gather x1, waiting for transfers between devices, per_device(): lax.all_gather(key_large, 'sp', axis=0, tiled=True)  61 us
    all_gather x1, waiting for transfers between devices, per_device(): lax.all_gather(value_large, 'sp', axis=0, tiled=True)  60.8 us
    all_gather x1, waiting for transfers between devices, per_device(): lax.all_gather(value_small, 'sp', axis=0, tiled=True)  53.8 us
    reduce_scatter x1, waiting for transfers between devices, per_device(): lax.psum_scatter(ffn_terms.astype(jnp.bfloat16), 'tp', scatter_dimension=...  36.2 us
    all_gather x1, blocking collectives, per_device(): lax.all_gather(gates_large, 'sp', axis=0, tiled=True)  33.1 us
  transfers between devices with their start and end apart: 12, of which 9 were waited for; matrix products, arithmetic and copies ran while one was open for 8% of the time, Pallas kernels for 0%

profile of v1, /device:TPU:0, one launch (start us, length us, event | category | flops | bytes accessed | tf_op | source)
XLA Modules:
  0.0 725.4 jit_solution(9451373479399422481)
XLA Ops:
  16.8 33.1 %all_gather.43 = f32[6144,2]{0,1:T(2,128)S(1)} all-gather(f32[768,2]{0,1:T(2,128)S(1)} %copy-done.5), channel_id=1, replica_groups=mesh['sp'=8,'tp'=4] {'sp'}, dimensions={0}, use_global_device_ids=true | all-gather | bytes 55296 | tf_op jit(solution)/shard_map/all_gather | solution.py:95
  49.9 31.3 %all_gather.40 = f32[6144,4]{0,1:T(4,128)S(1)} all-gather(f32[768,4]{0,1:T(4,128)S(1)} %copy-done.3), channel_id=1, replica_groups=mesh['sp'=8,'tp'=4] {'sp'}, dimensions={0}, use_global_device_ids=true | all-gather | bytes 110592 | tf_op jit(solution)/shard_map/all_gather | solution.py:94
  81.2 53.8 %all-gather.14.cloned.1.call-done = bf16[6144,256]{0,1:T(8,128)(2,1)} async-done(((bf16[768,256]{0,1:T(8,128)(2,1)}), bf16[6144,256]{0,1:T(8,128)(2,1)}) %all-gather.14.cloned.1.call-update) | async-done | bytes 3145744 | tf_op jit(solution)/shard_map/all_gather | solution.py:109
  135.0 61.0 %all-gather.16.cloned.1.call-done = bf16[6144,256]{0,1:T(8,128)(2,1)} async-done(((bf16[768,256]{0,1:T(8,128)(2,1)}), bf16[6144,256]{0,1:T(8,128)(2,1)}) %all-gather.16.cloned.1.call-update) | async-done | bytes 3145744 | tf_op jit(solution)/shard_map/all_gather | solution.py:110
  196.0 60.8 %all-gather.18.cloned.1.call-done = bf16[6144,256]{0,1:T(8,128)(2,1)} async-done(((bf16[768,256]{0,1:T(8,128)(2,1)}), bf16[6144,256]{0,1:T(8,128)(2,1)}) %all-gather.18.cloned.1.call-update) | async-done | bytes 3145744 | tf_op jit(solution)/shard_map/all_gather | solution.py:111
  257.0 19.2 %while.24 = (s32[]{:T(128)}, f32[4,768]{1,0:T(4,128)S(1)}, f32[4,768]{1,0:T(4,128)S(1)}, f32[768,4,64]{0,2,1:T(8,128)S(1)}, f32[2,768]{1,0:T(2,128)S(1)}, /*inde...) while((s32[]{:T(128)}, f32[4,768]{1,0:T(4,128)S(1)}, ...), condition=%wide.region_7.8_spmd.clone, body=%wide.region_0.7_spmd.clone.sunk | while | flops 1276591104 | bytes 55708176 | solution.py:154
  257.0 18.5 %conditional.3 = ((f32[4,768]{1,0:T(4,128)S(1)}, f32[4,768]{1,0:T(4,128)S(1)}, f32[768,4,64]{0,2,1:T(8,128)S(1)}, f32[2,768]{1,0:T(2,128)S(1)}, f32[2,768]{1,0:T(2,128)S(1)}, /*index=5*/f32[768,2,128]{2,0,1:T(8,128)S(1)})) conditional(s32[]{:T(128)} %convert_element_type.127, (f32[4,768]{1,0:T(4,128)S(1)}, f32[4,768]{1,0:T(4,128)S(1)}, ...), branch_computations={%region_1.0_spmd, %region_2.6_spmd} | conditional | flops 1276591104 | bytes 55704688 | solution.py:151
  265.7 2.7 fusion.4
  268.5 3.6 fusion.23
  272.1 3.5 fusion.3
  279.1 19.0 %all_to_all.13 = bf16[4,192,512]{2,1,0:T(8,128)(2,1)S(1)} all-to-all(bf16[4,192,512]{2,1,0:T(8,128)(2,1)S(1)} %copy.66), channel_id=1, replica_groups=mesh['sp'=8,'tp'=4] {'tp'}, dimensions={0} | all-to-all | bytes 1572864 | tf_op jit(solution)/shard_map/all_to_all | solution.py:170
  298.3 3.5 fusion.49
  301.8 26.3 %all-gather.22.cloned.1.call-done = bf16[1024,2048]{1,0:T(8,128)(2,1)} async-done(((bf16[256,2048]{1,0:T(8,128)(2,1)}), bf16[1024,2048]{1,0:T(8,128)(2,1)}) %all-gather.22.cloned.1.call-update) | async-done | bytes 4194320 | tf_op jit(solution)/shard_map/all_gather | solution.py:181
  328.0 3.6 fusion.48
  334.5 92.1 %all-gather.26.cloned.1.call-done = bf16[2048,1408]{1,0:T(8,128)(2,1)} async-done(((bf16[256,1408]{1,0:T(8,128)(2,1)}), bf16[2048,1408]{1,0:T(8,128)(2,1)}) %all-gather.26.cloned.1.call-update) | async-done | bytes 5767184 | tf_op jit(solution)/shard_map/all_gather | solution.py:197
  426.7 30.8 %all-gather.24.cloned.1.call-done = bf16[768,2048]{1,0:T(8,128)(2,1)} async-done(((bf16[192,2048]{1,0:T(8,128)(2,1)}), bf16[768,2048]{1,0:T(8,128)(2,1)}) %all-gather.24.cloned.1.call-update) | async-done | bytes 3145744 | tf_op jit(solution)/shard_map/all_gather | solution.py:187
  457.4 8.3 %convolution_convert_fusion.2 = bf16[768,1408]{1,0:T(8,128)(2,1)S(1)} fusion(bf16[768,2048]{1,0:T(8,128)(2,1)} %all-gather.24.cloned.1.call-done, bf16[2048,1408]{1,0:T(8,128)(2,1)} %all-gather.26.cloned.1.call-done), kind=kOutput, calls=%fused_computation.57 | convolution fusion | flops 4430266368 | bytes 11075584 | tf_op jit(solution)/shard_map/dot_general | solution.py:191
  467.2 84.8 %all-gather.28.cloned.1.call-done = bf16[2048,1408]{1,0:T(8,128)(2,1)} async-done(((bf16[256,1408]{1,0:T(8,128)(2,1)}), bf16[2048,1408]{1,0:T(8,128)(2,1)}) %all-gather.28.cloned.1.call-update) | async-done | bytes 5767184 | tf_op jit(solution)/shard_map/all_gather | solution.py:198
  552.0 8.3 %convolution_convert_fusion.1 = bf16[768,1408]{1,0:T(8,128)(2,1)S(1)} fusion(bf16[768,2048]{1,0:T(8,128)(2,1)} %all-gather.24.cloned.1.call-done, bf16[2048,1408]{1,0:T(8,128)(2,1)} %all-gather.28.cloned.1.call-done), kind=kOutput, calls=%fused_computation.56 | convolution fusion | flops 4430266368 | bytes 11075584 | tf_op jit(solution)/shard_map/dot_general | solution.py:192
  564.3 80.5 %all-gather.30.cloned.1.call-done = bf16[11264,256]{1,0:T(8,128)(2,1)} async-done(((bf16[1408,256]{1,0:T(8,128)(2,1)}), bf16[11264,256]{1,0:T(8,128)(2,1)}) %all-gather.30.cloned.1.call-update) | async-done | bytes 5767184 | tf_op jit(solution)/shard_map/all_gather | solution.py:14
  644.8 8.3 %copy.69 = bf16[1408,8,256]{0,2,1:T(8,128)(2,1)} copy(bf16[1408,8,256]{2,0,1:T(8,128)(2,1)} %bitcast.93) | data formatting | bytes 11534336 | tf_op jit(solution)/shard_map/reshape | solution.py:15
  653.0 6.5 maximum_convert_fusion
  659.6 17.7 %convolution_convert_fusion = bf16[768,2048]{1,0:T(8,128)(2,1)} fusion(bf16[1408,2048]{0,1:T(8,128)(2,1)} %bitcast.94, f32[770,1408]{1,0:T(8,128)} %get-tuple-element.745, f32[770,1408]{1,0:T(8,128)} %get-tuple-element.744, f32[1408]{0:T(1024)S(1)} %get-tuple-element.684, f32[1408]{0:T(1024)S(1)} %get-tuple-element.685, f32[1408]{0:T(1024)S(1)} %get-tuple-element.683, ...), kind=kOutput, calls=%fused_computation.55 | convolution fusion | flops 4448059392 | bytes 34898944 | tf_op jit(solution)/shard_map/dot_general | solution.py:221
  677.3 36.2 %reduce-scatter.2.cloned.1.call-done = bf16[192,2048]{1,0:T(8,128)(2,1)} async-done(((bf16[768,2048]{1,0:T(8,128)(2,1)}), bf16[192,2048]{1,0:T(8,128)(2,1)}) %reduce-scatter.2.cloned.1.call-update) | async-done | bytes 786448 | tf_op jit(solution)/shard_map/reduce_scatter | solution.py:224
  (113 shorter events, 35.5 us)
Async XLA Ops:
  6.5 10.1 %copy-start.4 = (bf16[768,256]{1,0:T(8,128)(2,1)S(1)}, bf16[768,256]{1,0:T(8,128)(2,1)}, u32[]{:S(2)}) copy-start(bf16[768,256]{1,0:T(8,128)(2,1)} %param.22) | copy-start | bytes 1179652
  6.5 10.2 %copy-start.5 = (f32[768,2]{0,1:T(2,128)S(1)}, f32[768,2]{0,1:T(2,128)}, u32[]{:S(2)}) copy-start(f32[768,2]{0,1:T(2,128)} %param.29) | copy-start | bytes 18436
  6.5 43.4 %copy-start.3 = (f32[768,4]{0,1:T(4,128)S(1)}, f32[768,4]{0,1:T(4,128)}, u32[]{:S(2)}) copy-start(f32[768,4]{0,1:T(4,128)} %param.25) | copy-start | bytes 36868
  6.5 74.7 %all-gather.12.cloned.1.call-start = ((), (), s32[]{:S(2)}) async-start(), calls=%async_computation.2 | async-start | bytes 3538944 | tf_op jit(solution)/shard_map/all_gather | solution.py:108
  8.5 248.5 %copy-start.10 = (bf16[768,256]{1,0:T(8,128)(2,1)S(1)}, bf16[768,256]{1,0:T(8,128)(2,1)}, u32[]{:S(2)}) copy-start(bf16[768,256]{1,0:T(8,128)(2,1)} %param.26) | copy-start | bytes 1179652
  8.5 126.5 %all-gather.14.cloned.1.call-start = ((), (), s32[]{:S(2)}) async-start(), calls=%async_computation.3 | async-start | bytes 3538944 | tf_op jit(solution)/shard_map/all_gather | solution.py:109
  10.6 185.4 %all-gather.16.cloned.1.call-start = ((), (), s32[]{:S(2)}) async-start(), calls=%async_computation.4 | async-start | bytes 3538944 | tf_op jit(solution)/shard_map/all_gather | solution.py:110
  12.6 244.2 %all-gather.18.cloned.1.call-start = ((), (), s32[]{:S(2)}) async-start(), calls=%async_computation.5 | async-start | bytes 3538944 | tf_op jit(solution)/shard_map/all_gather | solution.py:111
  14.6 283.6 %all-gather.20.cloned.1.call-start = ((), (), s32[]{:S(2)}) async-start(), calls=%async_computation.6 | async-start | bytes 5242880 | tf_op jit(solution)/shard_map/all_gather | solution.py:177
  15.2 312.8 %all-gather.22.cloned.1.call-start = ((), (), s32[]{:S(2)}) async-start(), calls=%async_computation.7 | async-start | bytes 5242880 | tf_op jit(solution)/shard_map/all_gather | solution.py:181
  15.8 410.9 %all-gather.26.cloned.1.call-start = ((), (), s32[]{:S(2)}) async-start(), calls=%async_computation.9 | async-start | bytes 6488064 | tf_op jit(solution)/shard_map/all_gather | solution.py:197
  16.5 440.9 %all-gather.24.cloned.1.call-start = ((), (), s32[]{:S(2)}) async-start(), calls=%async_computation.8 | async-start | bytes 3932160 | tf_op jit(solution)/shard_map/all_gather | solution.py:187
  328.0 3.9 copy-start.6
  333.2 218.8 %all-gather.28.cloned.1.call-start = ((), (), s32[]{:S(2)}) async-start(), calls=%async_computation.10 | async-start | bytes 6488064 | tf_op jit(solution)/shard_map/all_gather | solution.py:198
  333.9 310.8 %all-gather.30.cloned.1.call-start = ((), (), s32[]{:S(2)}) async-start(), calls=%async_computation.12 | async-start | bytes 6488064 | tf_op jit(solution)/shard_map/all_gather | solution.py:14
  334.5 379.1 %reduce-scatter.2.cloned.1.call-start = ((), (), s32[]{:S(2)}) async-start(), calls=%async_computation.11 | async-start | bytes 3932160 | tf_op jit(solution)/shard_map/reduce_scatter | solution.py:224
  465.8 1.4 copy-start.1
  467.2 97.0 %copy-start.7 = (f32[3,1408]{1,0:T(4,128)S(1)}, f32[3,1408]{1,0:T(4,128)}, u32[]{:S(2)}) copy-start(f32[3,1408]{1,0:T(4,128)} %param.36) | copy-start | bytes 50692
  467.2 97.0 %copy-start.8 = (f32[3,1408]{1,0:T(4,128)S(1)}, f32[3,1408]{1,0:T(4,128)}, u32[]{:S(2)}) copy-start(f32[3,1408]{1,0:T(4,128)} %param.37) | copy-start | bytes 50692
  560.3 1.3 copy-start.2
  561.7 91.3 %collective-permute-start = (bf16[2,2816]{1,0:T(2,128)(2,1)S(1)}, bf16[2,2816]{1,0:T(2,128)(2,1)S(1)}, u32[]{:S(2)}, u32[]{:S(2)}) collective-permute-start(bf16[2,2816]{1,0:T(2,128)(2,1)S(1)} %pad_maximum_fusion.1), channel_id=1, source_target_pairs={{0,4},{4,8},{8,12},{12,16},{16,20},{20,24},{24,28},{1,5},{5,9},{9,... | collective-permute-start | bytes 33800 | tf_op jit(solution)/shard_map/ppermute | solution.py:22
  677.3 39.7 %copy-start.9 = (f32[2048]{0:T(1024)S(1)}, f32[2048]{0:T(1024)}, u32[]{:S(2)}) copy-start(f32[2048]{0:T(1024)} %param.39) | copy-start | bytes 24580
  713.6 3.5 copy-start
Sparse Core Ops, SparseCore 0:
  9.6 64.2 all-gather.11
  76.1 58.8 all-gather.13
  137.3 58.6 all-gather.15
  198.1 58.6 all-gather.17
  258.2 37.8 all-gather.19
  297.5 30.4 all-gather.21
  330.2 96.3 all-gather.25
  428.2 29.1 all-gather.23
  459.6 92.2 all-gather.27
  554.0 90.7 all-gather.29
  677.5 36.0 reduce-scatter.1
